TPU v7x, 32 devices: a whole 2x2x4 slice. The times are simulated.
32 devices in a mesh: rep: 8 (over z, y), fs: 2 (over x), tp: 2 (over core).
Axes of the slice: x: 2, y: 2, z: 4, core: 2. Of those that a mesh axis runs over, the one named last changes fastest.
Arguments:
- tokens: bfloat16 [8192, 1024], P(('rep', 'fs', 'tp')), may hold values from -6 to 6
- cotangent: bfloat16 [8192, 1024], P(('rep', 'fs', 'tp')), may hold values from -8 to 8
- gate_weight: bfloat16 [1024, 2816], P(None, ('fs', 'tp')), may hold values from -0.1875 to 0.1875
- value_weight: bfloat16 [1024, 2816], P(None, ('fs', 'tp')), may hold values from -0.1875 to 0.1875
- down_weight: bfloat16 [2816, 1024], P(('fs', 'tp')), may hold values from -0.109375 to 0.109375
- gate_taps: float32 [3, 2816], P(None, ('fs', 'tp')), may hold values from -3.5 to 3.5
- value_taps: float32 [3, 2816], P(None, ('fs', 'tp')), may hold values from -3.5 to 3.5
Outputs:
- input_grad: bfloat16 [8192, 1024], P(('rep', 'fs', 'tp'))
- gate_grad: float32 [1024, 2816], P(None, ('fs', 'tp'))
- value_grad: float32 [1024, 2816], P(None, ('fs', 'tp'))
- down_grad: float32 [2816, 1024], P(('fs', 'tp'))
- gate_taps_grad: float32 [3, 2816], P(None, ('fs', 'tp'))
- value_taps_grad: float32 [3, 2816], P(None, ('fs', 'tp'))
All inputs are finite; a program needn't handle non-finite values.
Results may differ from a plain program's by a relative error of at most 0.0062.
Values may be sent and summed in bfloat16 or wider, within the bound.
A program may use at most 128 MiB of HBM per device.

v0:
```python
import math

import jax
import jax.numpy as jnp
from jax import lax
from jax.sharding import PartitionSpec as P


def shift_back(field, offset):
    return jnp.pad(field, ((offset, 0), (0, 0)))[: field.shape[0]]


def shift_ahead(field, offset):
    return jnp.pad(field, ((0, offset), (0, 0)))[offset:]


def causal_mix(field, taps):
    total = taps[0][None, :] * field
    for offset in range(1, taps.shape[0]):
        total = total + taps[offset][None, :] * shift_back(field, offset)
    return total


def reverse_mix(field, taps):
    total = taps[0][None, :] * field
    for offset in range(1, taps.shape[0]):
        total = total + taps[offset][None, :] * shift_ahead(field, offset)
    return total


def tap_sums(back, field, count):
    return jnp.stack([jnp.sum(back * shift_back(field, offset), axis=0) for offset in range(count)])


def contract_rows(left, right):
    return lax.dot_general(
        left, right, (((0,), (0,)), ((), ())), preferred_element_type=jnp.float32
    )


def contract_cols(left, right):
    return lax.dot_general(
        left, right, (((1,), (1,)), ((), ())), preferred_element_type=jnp.float32
    )


def per_device(tokens, cotangent, gate_weight, value_weight, down_weight, gate_taps, value_taps):
    local_rows = tokens.shape[0]
    hidden_cols = gate_weight.shape[1]
    seq_len = local_rows * lax.axis_size("fs") * lax.axis_size("tp")
    total_tokens = seq_len * lax.axis_size("rep")
    scale = 1.0 / math.sqrt(total_tokens)
    both_weights = jnp.concatenate([gate_weight, value_weight], axis=1)
    piece = lax.all_gather(tokens, ("fs", "tp"), axis=0, tiled=True)
    whole = piece
    block = jnp.dot(piece, both_weights, preferred_element_type=jnp.float32).astype(jnp.bfloat16)
    projected = block
    token_whole, projected = (whole, projected)
    piece = lax.all_gather(cotangent, ("fs", "tp"), axis=0, tiled=True)
    whole = piece
    back = contract_cols(piece, down_weight)
    up_gate = projected[:, :hidden_cols].astype(jnp.float32)
    up_value = projected[:, hidden_cols:].astype(jnp.float32)
    conv_gate = causal_mix(up_gate, gate_taps)
    conv_value = causal_mix(up_value, value_taps)
    sigma = jax.nn.sigmoid(conv_gate)
    silu_gate = conv_gate * sigma
    hidden = (silu_gate * conv_value).astype(jnp.bfloat16)
    back_value = back * silu_gate
    back_gate = back * conv_value * sigma * (1.0 + conv_gate * (1.0 - sigma))
    grad_gate = reverse_mix(back_gate, gate_taps).astype(jnp.bfloat16)
    grad_value = reverse_mix(back_value, value_taps).astype(jnp.bfloat16)
    tap_count = gate_taps.shape[0]
    input_grad = lax.psum_scatter(
        contract_cols(grad_gate, gate_weight) + contract_cols(grad_value, value_weight),
        ("fs", "tp"),
        scatter_dimension=0,
        tiled=True,
    ).astype(jnp.bfloat16)
    gate_part = contract_rows(token_whole, grad_gate)
    value_part = contract_rows(token_whole, grad_value)
    down_part = contract_rows(hidden, whole)
    gate_tap_part = tap_sums(back_gate, up_gate, tap_count)
    value_tap_part = tap_sums(back_value, up_value, tap_count)
    summed = lax.psum((gate_part, value_part, down_part, gate_tap_part, value_tap_part), "rep")
    weight_out = tuple((item * scale for item in summed))
    return (input_grad, weight_out[0], weight_out[1], weight_out[2], weight_out[3], weight_out[4])


def solution(mesh):
    in_specs = (
        P(("rep", "fs", "tp"), None),
        P(("rep", "fs", "tp"), None),
        P(None, ("fs", "tp")),
        P(None, ("fs", "tp")),
        P(("fs", "tp"), None),
        P(None, ("fs", "tp")),
        P(None, ("fs", "tp")),
    )
    out_specs = (
        P(("rep", "fs", "tp"), None),
        P(None, ("fs", "tp")),
        P(None, ("fs", "tp")),
        P(("fs", "tp"), None),
        P(None, ("fs", "tp")),
        P(None, ("fs", "tp")),
    )
    return jax.shard_map(
        per_device, mesh=mesh, in_specs=in_specs, out_specs=out_specs, check_vma=False
    )
```

profile of v0, /device:TPU:24, one launch (start us, length us, event | category | flops | bytes accessed | tf_op | source)
XLA Modules:
  0.0 436.9 jit_solution(10589605548296215302)
XLA Ops:
  7.2 0.0 copy-start
  7.2 0.0 all-gather.5.cloned.1.call-start
  7.2 0.7 all-gather.5.cloned.1.call-update
  7.9 0.0 all-gather.3.cloned.1.call-start
  8.0 0.7 all-gather.3.cloned.1.call-update
  8.7 0.0 reduce-scatter.2.cloned.1.call-start
  8.7 0.8 slice_reduce_fusion.5
  9.6 0.8 slice_reduce_fusion.4
  10.4 22.7 %all-gather.5.cloned.1.call-done = bf16[1024,1024]{1,0:T(8,128)(2,1)} async-done(((bf16[256,1024]{1,0:T(8,128)(2,1)}), bf16[1024,1024]{1,0:T(8,128)(2,1)}) %all-gather.5.cloned.1.call-update) | async-done | bytes 2097168 | tf_op jit(solution)/shard_map/all_gather | solution.py:54
  33.1 5.7 %fusion = bf16[1024,1408]{0,1:T(8,128)(2,1)S(1)} fusion(bf16[1024,1024]{1,0:T(8,128)(2,1)} %all-gather.5.cloned.1.call-done, bf16[1024,704]{0,1:T(8,128)(2,1)} %param.10, bf16[1024,704]{0,1:T(8,128)(2,1)} %param.9), kind=kOutput, calls=%fused_computation.1 | convolution fusion | flops 2959998976 | bytes 7864320 | tf_op jit(solution)/shard_map/dot_general | solution.py:56
  38.8 0.0 copy-start.4
  38.8 1.6 copy-done.4
  40.4 3.2 slice_convert_fusion.1
  43.6 13.7 %all-gather.3.cloned.1.call-done = bf16[1024,1024]{1,0:T(8,128)(2,1)} async-done(((bf16[256,1024]{1,0:T(8,128)(2,1)}), bf16[1024,1024]{1,0:T(8,128)(2,1)}) %all-gather.3.cloned.1.call-update) | async-done | bytes 2097168 | tf_op jit(solution)/shard_map/all_gather | solution.py:59
  57.3 0.0 copy-done
  57.3 23.6 %multiply_reduce_fusion.2 = (f32[704]{0:T(1024)S(1)}, f32[704]{0:T(1024)S(1)}, f32[704]{0:T(1024)S(1)}, f32[704]{0:T(1024)S(1)}, f32[704]{0:T(1024)S(1)}, /*inde...) fusion(bf16[1024,1408]{0,1:T(8,128)(2,1)} %copy-done.4, ...), kind=kOutput, calls=%fused_computation.25 | convolution fusion | flops 1501621760 | bytes 23757824 | tf_op jit(solution)/shard_map/dot_general | solution.py:42
  80.9 0.0 copy-start.7
  80.9 11.0 %fusion.4 = (bf16[1024,704]{0,1:T(8,128)(2,1)S(1)}, bf16[1024,704]{0,1:T(8,128)(2,1)S(1)}) fusion(f32[1024,704]{0,1:T(8,128)} %get-tuple-element.28, f32[704]{0:T(1024)S(1)} %get-tuple-element.20, f32[704]{0:T(1024)S(1)} %get-tuple-element.21, f32[704]{0:T(1024)S(1)} %get-tuple-element.19, f32[1024,704]{0,1:T(8,128)} %get-tuple-element.27, ...), kind=kLoop, calls=%fused_computation.13 | loop fusion | flops 8650752 | bytes 8667648 | tf_op jit(solution)/shard_map/convert_element_type | solution.py:71
  91.9 0.0 copy-done.7
  92.0 0.0 copy-start.8
  92.0 1.9 fusion.21
  93.8 0.0 copy-done.8
  93.8 3.8 convolution_add_fusion
  97.7 0.0 reduce-scatter.2.cloned.1.call-update
  97.7 0.2 all-reduce.12.cloned.1.call-start
  97.9 0.0 copy-start.5
  97.9 5.0 %convolution_bitcast_fusion.1 = f32[1024,704]{0,1:T(8,128)} fusion(bf16[1024,704]{0,1:T(8,128)(2,1)S(1)} %get-tuple-element.33, bf16[1024,1024]{1,0:T(8,128)(2,1)} %all-gather.5.cloned.1.call-done), kind=kOutput, calls=%fused_computation.37 | convolution fusion | flops 1476395008 | bytes 6422528 | tf_op jit(solution)/shard_map/dot_general | solution.py:36
  102.9 0.0 copy-done.5
  102.9 0.0 copy-start.6
  102.9 0.0 copy-start.9
  102.9 0.0 copy-start.10
  102.9 3.3 convolution_bitcast_fusion
  106.2 0.0 copy-done.6
  106.2 0.3 copy-done.9
  106.5 1.9 copy-done.10
  108.4 3.3 fusion.15
  111.7 0.0 all-reduce.12.cloned.1.call-update
  111.9 32.5 %all-reduce.8 = (f32[3,704]{1,0:T(4,128)S(1)}, f32[3,704]{1,0:T(4,128)S(1)}) all-reduce(f32[3,704]{1,0:T(4,128)S(1)} %pad_maximum_fusion, f32[3,704]{1,0:T(4,128)S(1)} %pad_maximum_fusion.1), channel_id=1, replica_groups=mesh['rep'=8,'fs'=2,'tp'=2] {'rep'}, use_global_device_ids=true, to_apply=%region_7.8 | all-reduce | flops 4224 | bytes 33792 | tf_op jit(solution)/shard_map/psum | solution.py:85
  144.4 0.6 broadcast_multiply_fusion.3
  145.0 0.0 reduce-scatter.2.cloned.1.call-done
  145.0 2.1 convert_element_type.46
  147.1 274.4 %all-reduce.12.cloned.1.call-done = (f32[1024,704]{0,1:T(8,128)}, f32[1024,704]{0,1:T(8,128)}, f32[704,1024]{1,0:T(8,128)}) async-done(((f32[1024,704]{0,1:T(8,128)}, f32[1024,704]{0,1:T(8,128)}, f32[704,1024]{1,0:T(8,128)}), (f32[1024,704]{0,1:T(8,128)}, f32[1024,704]{0,1:T(8,128)}, f32[704,1024]{1,0:T(8,128)})) %all-reduce.12.cloned.1.call-update) | async-done | bytes 8650768 | tf_op jit(solution)/shard_map/psum | solution.py:85
  421.5 4.1 broadcast_multiply_fusion.2
  425.6 0.0 copy-done.3
  425.6 1.9 broadcast_multiply_fusion.1
  427.5 1.0 copy-done.2
  428.5 1.9 broadcast_multiply_fusion
  430.4 0.0 copy-done.1
  (11 shorter events, 0.1 us)
Async XLA Ops:
  7.2 50.1 %copy-start = (bf16[704,1024]{1,0:T(8,128)(2,1)S(1)}, bf16[704,1024]{1,0:T(8,128)(2,1)}, u32[]{:S(2)}) copy-start(bf16[704,1024]{1,0:T(8,128)(2,1)} %param.11) | copy-start | bytes 4325380
  7.2 25.9 %all-gather.5.cloned.1.call-start = ((), (), s32[]{:S(2)}) async-start(), calls=%async_computation.2 | async-start | bytes 2621440 | tf_op jit(solution)/shard_map/all_gather | solution.py:54
  7.9 49.4 %all-gather.3.cloned.1.call-start = ((), (), s32[]{:S(2)}) async-start(), calls=%async_computation.1 | async-start | bytes 2621440 | tf_op jit(solution)/shard_map/all_gather | solution.py:59
  8.7 136.3 %reduce-scatter.2.cloned.1.call-start = ((), (), s32[]{:S(2)}) async-start(), calls=%async_computation.3 | async-start | bytes 5242880 | tf_op jit(solution)/shard_map/reduce_scatter | solution.py:74
  38.8 1.6 copy-start.4
  80.9 11.0 %copy-start.7 = (bf16[1024,704]{0,1:T(8,128)(2,1)S(1)}, bf16[1024,704]{0,1:T(8,128)(2,1)}, u32[]{:S(2)}) copy-start(bf16[1024,704]{0,1:T(8,128)(2,1)} %param.9) | copy-start | bytes 4325380
  92.0 1.9 copy-start.8
  97.7 323.8 %all-reduce.12.cloned.1.call-start = ((), (), s32[]{:S(2)}) async-start(), calls=%async_computation.4 | async-start | bytes 17301504 | tf_op jit(solution)/shard_map/psum | solution.py:85
  97.9 5.0 %copy-start.5 = (bf16[1024,1024]{1,0:T(8,128)(2,1)S(1)}, bf16[1024,1024]{1,0:T(8,128)(2,1)}, u32[]{:S(2)}) copy-start(bf16[1024,1024]{1,0:T(8,128)(2,1)} %all-gather.5.cloned.1.call-done) | copy-start | bytes 6291460
  102.9 3.3 copy-start.6
  102.9 3.6 copy-start.9
  102.9 5.5 %copy-start.10 = (f32[1024,704]{0,1:T(8,128)S(1)}, f32[1024,704]{0,1:T(8,128)}, u32[]{:S(2)}) copy-start(f32[1024,704]{0,1:T(8,128)} %get-tuple-element.30) | copy-start | bytes 8650756
  421.5 4.1 copy-start.3
  425.6 2.9 copy-start.2
  427.5 2.9 copy-start.1
Sparse Core Ops, SparseCore 0:
  9.5 23.5 all-gather.4
  34.7 22.5 all-gather.2
  97.8 44.5 reduce-scatter.1
  147.2 274.2 all-reduce.11
where the time goes:
time: 441 us; the launch traced here: 437 us
  waiting for transfers between devices  312 us (71%)
  matrix products  46.5 us (11%)
  blocking collectives  32.5 us (7%)
  other arithmetic  24.9 us (6%)
  between operations  13.9 us (3%)
  local copies, waits for them, and re-layouts  6.5 us (1%)
    psum x1, waiting for transfers between devices, per_device(): lax.psum((gate_part, value_part, down_part, gate_tap_part, value_tap_part...  274 us
    psum x1, blocking collectives, per_device(): lax.psum((gate_part, value_part, down_part, gate_tap_part, value_tap_part...  32.5 us
    dot_general x3, matrix products, contract_cols(): lax.dot_general(left, right, (((1,), (1,)), ((), ())), preferred_element_...  29.3 us
    all_gather x1, waiting for transfers between devices, per_device(): piece = lax.all_gather(tokens, ('fs', 'tp'), axis=0, tiled=True)  22.7 us
    all_gather x1, waiting for transfers between devices, per_device(): piece = lax.all_gather(cotangent, ('fs', 'tp'), axis=0, tiled=True)  13.7 us
    dot_general x3, matrix products, contract_rows(): lax.dot_general(left, right, (((0,), (0,)), ((), ())), preferred_element_...  11.6 us
    convert_element_type x1, other arithmetic, per_device(): grad_gate = reverse_mix(back_gate, gate_taps).astype(jnp.bfloat16)  11 us
  transfers between devices with their start and end apart: 4, of which 3 were waited for; matrix products, arithmetic and copies ran while one was open for 6% of the time, Pallas kernels for 0%

commit v1 on v0

--- a/solution.py
+++ b/solution.py
@@ -1,8 +1,11 @@
+import functools
 import math
 
 import jax
 import jax.numpy as jnp
 from jax import lax
+from jax.experimental import pallas as pl
+from jax.experimental.pallas import tpu as pltpu
 from jax.sharding import PartitionSpec as P
 
 
@@ -41,6 +44,182 @@
 def contract_cols(left, right):
     return lax.dot_general(
         left, right, (((1,), (1,)), ((), ())), preferred_element_type=jnp.float32
+    )
+
+MESH = pl.DeviceIdType.MESH
+
+
+def send(src, dst, send_sem, recv_sem, where):
+    return pltpu.make_async_remote_copy(
+        src_ref=src, dst_ref=dst, send_sem=send_sem, recv_sem=recv_sem, device_id=where, device_id_type=MESH
+    )
+
+
+def reduce_kernel(
+    n, fs, tp, scale,
+    gv, dn, ig, taps,
+    gv_out, dn_out, ig_out, taps_out,
+    gv_y, dn_y, gv_z, dn_z, gv_in, dn_in, ig_in, taps_in,
+    y_send, y_recv, z_send, z_recv, az_send, az_recv, ay_send, ay_recv, ig_send, ig_recv, t_send, t_recv,
+):
+    depth = n // 2
+    me = lax.axis_index("rep")
+    y, z = lax.rem(me, 2), lax.div(me, 2)
+    partner = me + 1 - 2 * y
+    my_fs, my_tp = lax.axis_index("fs"), lax.axis_index("tp")
+    rows = gv.shape[0] // n
+    cols = dn.shape[1] // n
+    group = fs * tp
+    ig_rows = ig.shape[0] // group
+    mine = my_fs * tp + my_tp
+
+    def gv_rows(chunk):
+        return pl.ds(pl.multiple_of(chunk * rows, rows), rows)
+
+    def dn_cols(chunk):
+        return pl.ds(pl.multiple_of(chunk * cols, cols), cols)
+
+    def mate(offset):
+        spot = lax.rem(mine + offset, group)
+        return spot, {"fs": lax.div(spot, tp), "tp": lax.rem(spot, tp)}
+
+    barrier = pltpu.get_barrier_semaphore()
+    for offset in range(1, n):
+        pl.semaphore_signal(barrier, inc=1, device_id={"rep": lax.rem(me + offset, n)}, device_id_type=MESH)
+    for offset in range(1, group):
+        pl.semaphore_signal(barrier, inc=1, device_id=mate(offset)[1], device_id_type=MESH)
+    pl.semaphore_wait(barrier, n - 1 + group - 1)
+
+    order = list(range(1, depth)) + [0]
+    first = []
+    for k in order:
+        zt = lax.rem(z + k, depth)
+        theirs = 2 * zt + 1 - y
+        pair = (
+            send(gv.at[gv_rows(theirs), :], gv_y.at[k], y_send.at[0, k], y_recv.at[0, k], {"rep": partner}),
+            send(dn.at[:, dn_cols(theirs)], dn_y.at[k], y_send.at[1, k], y_recv.at[1, k], {"rep": partner}),
+        )
+        for c in pair:
+            c.start()
+        first.append(pair)
+    igs = []
+    for offset in range(1, group):
+        spot, where = mate(offset)
+        c = send(
+            ig.at[pl.ds(pl.multiple_of(spot * ig_rows, ig_rows), ig_rows), :], ig_in.at[offset - 1],
+            ig_send.at[offset - 1], ig_recv.at[offset - 1], where,
+        )
+        c.start()
+        igs.append(c)
+    tcs = []
+    for offset in range(1, n):
+        c = send(taps, taps_in.at[me], t_send.at[offset - 1], t_recv.at[offset - 1], {"rep": lax.rem(me + offset, n)})
+        c.start()
+        tcs.append(c)
+
+    second = []
+    for i, k in enumerate(order):
+        zt = lax.rem(z + k, depth)
+        ours = 2 * zt + y
+        first[i][0].wait_recv()
+        gv_z[k] = (gv[gv_rows(ours), :].astype(jnp.float32) + gv_y[k].astype(jnp.float32)).astype(jnp.bfloat16)
+        first[i][1].wait_recv()
+        dn_z[k] = (dn[:, dn_cols(ours)].astype(jnp.float32) + dn_y[k].astype(jnp.float32)).astype(jnp.bfloat16)
+        if k:
+            where = {"rep": ours}
+            pair = (
+                send(gv_z.at[k], gv_in.at[k], z_send.at[0, k], z_recv.at[0, k], where),
+                send(dn_z.at[k], dn_in.at[k], z_send.at[1, k], z_recv.at[1, k], where),
+            )
+            for c in pair:
+                c.start()
+            second.append(pair)
+
+    for c in second:
+        c[0].wait_recv()
+        c[1].wait_recv()
+    gv_total = gv_z[0].astype(jnp.float32)
+    dn_total = dn_z[0].astype(jnp.float32)
+    for k in range(1, depth):
+        gv_total = gv_total + gv_in[k].astype(jnp.float32)
+        dn_total = dn_total + dn_in[k].astype(jnp.float32)
+    gv_out[gv_rows(me), :] = (gv_total * scale).astype(jnp.bfloat16)
+    dn_out[:, dn_cols(me)] = (dn_total * scale).astype(jnp.bfloat16)
+
+    def spread(chunk, k, sends, recvs, where):
+        pair = (
+            send(gv_out.at[gv_rows(chunk), :], gv_out.at[gv_rows(chunk), :], sends.at[0, k], recvs.at[0, k], where),
+            send(dn_out.at[:, dn_cols(chunk)], dn_out.at[:, dn_cols(chunk)], sends.at[1, k], recvs.at[1, k], where),
+        )
+        for c in pair:
+            c.start()
+        return pair
+
+    third = [spread(me, k, az_send, az_recv, {"rep": 2 * lax.rem(z + k, depth) + y}) for k in range(1, depth)]
+    last = [spread(me, 0, ay_send, ay_recv, {"rep": partner})]
+
+    for c in igs:
+        c.wait_recv()
+    own = ig[pl.ds(pl.multiple_of(mine * ig_rows, ig_rows), ig_rows), :].astype(jnp.float32)
+    for slot in range(group - 1):
+        own = own + ig_in[slot].astype(jnp.float32)
+    ig_out[...] = own.astype(jnp.bfloat16)
+    for c in tcs:
+        c.wait_recv()
+    taps_in[me] = taps[...]
+    total = taps_in[0]
+    for slot in range(1, n):
+        total = total + taps_in[slot]
+    taps_out[...] = total * scale
+
+    for k in range(1, depth):
+        third[k - 1][0].wait_recv()
+        third[k - 1][1].wait_recv()
+        last.append(spread(2 * lax.rem(z + depth - k, depth) + y, k, ay_send, ay_recv, {"rep": partner}))
+    for pair in last:
+        for c in pair:
+            c.wait_recv()
+    for pair in first + second + third + last:
+        for c in pair:
+            c.wait_send()
+    for c in igs + tcs:
+        c.wait_send()
+
+
+def reduce_all(gv, dn, ig, taps, n, fs, tp, scale):
+    depth, group = n // 2, fs * tp
+    rows, width = gv.shape[0] // n, gv.shape[1]
+    cols, tall = dn.shape[1] // n, dn.shape[0]
+    bf16 = jnp.bfloat16
+    dma = pltpu.SemaphoreType.DMA
+    vmem = pl.BlockSpec(memory_space=pltpu.VMEM)
+    gv_slots = pltpu.VMEM((depth, rows, width), bf16)
+    dn_slots = pltpu.VMEM((depth, tall, cols), bf16)
+    return pl.pallas_call(
+        functools.partial(reduce_kernel, n, fs, tp, scale),
+        out_shape=(
+            jax.ShapeDtypeStruct(gv.shape, bf16),
+            jax.ShapeDtypeStruct(dn.shape, bf16),
+            jax.ShapeDtypeStruct((ig.shape[0] // group, ig.shape[1]), bf16),
+            jax.ShapeDtypeStruct(taps.shape, jnp.float32),
+        ),
+        in_specs=[vmem] * 4,
+        out_specs=(vmem,) * 4,
+        scratch_shapes=[
+            gv_slots, dn_slots, gv_slots, dn_slots, gv_slots, dn_slots,
+            pltpu.VMEM((group - 1, ig.shape[0] // group, ig.shape[1]), bf16),
+            pltpu.VMEM((n,) + taps.shape, jnp.float32),
+        ] + [dma((2, depth))] * 8 + [dma((group - 1,))] * 2 + [dma((n - 1,))] * 2,
+        compiler_params=pltpu.CompilerParams(
+            collective_id=0, has_side_effects=True, vmem_limit_bytes=48 * 1024 * 1024
+        ),
+    )(gv, dn, ig, taps)
+
+
+def tiles_well(n, fs, tp, gv_rows, gv_cols, dn_rows, dn_cols):
+    return (
+        n % 2 == 0 and fs * tp > 1 and gv_rows % (16 * n) == 0 and gv_cols % 128 == 0
+        and dn_cols % (128 * n) == 0 and dn_rows % 16 == 0 and gv_rows % (16 * fs * tp) == 0
     )
 
 
@@ -71,6 +250,24 @@
     grad_gate = reverse_mix(back_gate, gate_taps).astype(jnp.bfloat16)
     grad_value = reverse_mix(back_value, value_taps).astype(jnp.bfloat16)
     tap_count = gate_taps.shape[0]
+    n, fs, tp = lax.axis_size("rep"), lax.axis_size("fs"), lax.axis_size("tp")
+    gate_tap_part = tap_sums(back_gate, up_gate, tap_count)
+    value_tap_part = tap_sums(back_value, up_value, tap_count)
+    if tiles_well(n, fs, tp, tokens.shape[1], 2 * hidden_cols, hidden_cols, cotangent.shape[1]):
+        grads = jnp.concatenate([grad_gate, grad_value], axis=1)
+        gv = contract_rows(token_whole, grads).astype(jnp.bfloat16)
+        dn = contract_rows(hidden, whole).astype(jnp.bfloat16)
+        ig = contract_cols(grads, both_weights).astype(jnp.bfloat16)
+        taps = jnp.pad(jnp.concatenate([gate_tap_part, value_tap_part], axis=1), ((0, -tap_count % 8), (0, 0)))
+        gv, dn, input_grad, taps = reduce_all(gv, dn, ig, taps, n, fs, tp, scale)
+        return (
+            input_grad,
+            gv[:, :hidden_cols].astype(jnp.float32),
+            gv[:, hidden_cols:].astype(jnp.float32),
+            dn.astype(jnp.float32),
+            taps[:tap_count, :hidden_cols],
+            taps[:tap_count, hidden_cols:],
+        )
     input_grad = lax.psum_scatter(
         contract_cols(grad_gate, gate_weight) + contract_cols(grad_value, value_weight),
         ("fs", "tp"),
@@ -80,8 +277,6 @@
     gate_part = contract_rows(token_whole, grad_gate)
     value_part = contract_rows(token_whole, grad_value)
     down_part = contract_rows(hidden, whole)
-    gate_tap_part = tap_sums(back_gate, up_gate, tap_count)
-    value_tap_part = tap_sums(back_value, up_value, tap_count)
     summed = lax.psum((gate_part, value_part, down_part, gate_tap_part, value_tap_part), "rep")
     weight_out = tuple((item * scale for item in summed))
     return (input_grad, weight_out[0], weight_out[1], weight_out[2], weight_out[3], weight_out[4])

time: 441 us -> 268 us (0.61)
  waiting for transfers between devices: 312 us -> 34 us
  Pallas kernels: 0 us -> 143 us
  blocking collectives: 32.5 us -> 0 us
  local copies, waits for them, and re-layouts: 6.5 us -> 15.4 us
  matrix products: 46.5 us -> 40.9 us
  other arithmetic: 24.9 us -> 19.6 us
    psum x1 -> x0, waiting for transfers between devices: 274 us -> none  [per_device(): lax.psum((gate_part, value_part, down_part, gate_tap_part, value_tap_part...]
    pallas_call x0 -> x1, Pallas kernels: none -> 143 us  [reduce_all(): pl.pallas_call(functools.partial(reduce_kernel, n, fs, tp, scale), out_sh...]
    psum x1 -> x0, blocking collectives: 32.5 us -> none  [per_device(): lax.psum((gate_part, value_part, down_part, gate_tap_part, value_tap_part...]
    mul x4 -> x0, other arithmetic: 8.52 us -> none  [per_device(): weight_out = tuple((item * scale for item in summed))]
    unnamed x22 -> x20, local copies, waits for them, and re-layouts: 4.78 us -> 11.8 us
    dot_general x3 -> x2, matrix products: 11.6 us -> 6.6 us  [contract_rows(): lax.dot_general(left, right, (((0,), (0,)), ((), ())), preferred_element_...]
    dot_general x3 -> x2, matrix products: 29.3 us -> 28.6 us  [contract_cols(): lax.dot_general(left, right, (((1,), (1,)), ((), ())), preferred_element_...]
  transfers between devices with their start and end apart: 4 -> 2, of which waited for: 3 -> 2; matrix products, arithmetic and copies ran while one was open for 6% -> 5% of each run, Pallas kernels for 0% -> 0%
where the time goes in v1:
time: 268 us
  Pallas kernels  143 us (53%)
  matrix products  40.9 us (15%)
  waiting for transfers between devices  34 us (13%)
  other arithmetic  19.6 us (7%)
  local copies, waits for them, and re-layouts  15.4 us (6%)
  between operations  14.2 us (5%)
    pallas_call x1, Pallas kernels, reduce_all(): pl.pallas_call(functools.partial(reduce_kernel, n, fs, tp, scale), out_sh...  143 us
    dot_general x2, matrix products, contract_cols(): lax.dot_general(left, right, (((1,), (1,)), ((), ())), preferred_element_...  28.6 us
    all_gather x1, waiting for transfers between devices, per_device(): piece = lax.all_gather(tokens, ('fs', 'tp'), axis=0, tiled=True)  19 us
    all_gather x1, waiting for transfers between devices, per_device(): piece = lax.all_gather(cotangent, ('fs', 'tp'), axis=0, tiled=True)  13.7 us
    unnamed x20, local copies, waits for them, and re-layouts  11.8 us
    convert_element_type x1, other arithmetic, per_device(): grad_gate = reverse_mix(back_gate, gate_taps).astype(jnp.bfloat16)  11 us
    dot_general x2, matrix products, contract_rows(): lax.dot_general(left, right, (((0,), (0,)), ((), ())), preferred_element_...  6.6 us
    dot_general x1, matrix products, per_device(): jnp.dot(piece, both_weights, preferred_element_type=jnp.float32)  5.65 us
  transfers between devices with their start and end apart: 2, of which 2 were waited for; matrix products, arithmetic and copies ran while one was open for 5% of the time, Pallas kernels for 0%

profile of v1, /device:TPU:24, one launch (start us, length us, event | category | flops | bytes accessed | tf_op | source)
XLA Modules:
  0.0 267.7 jit_solution(11899829078931756635)
XLA Ops:
  7.2 0.0 copy-start
  7.2 0.0 copy-start.3
  7.2 0.0 all-gather.5.cloned.1.call-start
  7.2 0.7 all-gather.5.cloned.1.call-update
  7.9 0.0 all-gather.3.cloned.1.call-start
  8.0 0.7 all-gather.3.cloned.1.call-update
  8.7 0.8 slice_reduce_fusion.5
  9.5 0.8 slice_reduce_fusion.4
  10.4 2.6 constant_dynamic-update-slice_fusion.1
  12.9 0.0 copy-done.3
  13.0 1.2 constant_dynamic-update-slice_fusion
  14.2 19.0 %all-gather.5.cloned.1.call-done = bf16[1024,1024]{1,0:T(8,128)(2,1)} async-done(((bf16[256,1024]{1,0:T(8,128)(2,1)}), bf16[1024,1024]{1,0:T(8,128)(2,1)}) %all-gather.5.cloned.1.call-update) | async-done | bytes 2097168 | tf_op jit(solution)/shard_map/all_gather | solution.py:233
  33.1 5.7 %fusion = bf16[1024,1408]{0,1:T(8,128)(2,1)S(1)} fusion(bf16[1024,1408]{0,1:T(8,128)(2,1)} %constant_dynamic-update-slice_fusion, bf16[1024,1024]{1,0:T(8,128)(2,1)} %all-gather.5.cloned.1.call-done), kind=kOutput, calls=%fused_computation.2 | convolution fusion | flops 2954231808 | bytes 7864320 | tf_op jit(solution)/shard_map/dot_general | solution.py:235
  38.8 0.0 copy-start.2
  38.8 1.6 copy-done.2
  40.4 3.2 %slice_convert_fusion.2 = (f32[1024,704]{0,1:T(8,128)}, f32[1024,704]{0,1:T(8,128)}) fusion(bf16[1024,1408]{0,1:T(8,128)(2,1)S(1)} %fusion), kind=kLoop, calls=%fused_computation.39 | loop fusion | flops 1441792 | bytes 8650752 | tf_op jit(solution)/shard_map/convert_element_type | solution.py:241
  43.6 13.7 %all-gather.3.cloned.1.call-done = bf16[1024,1024]{1,0:T(8,128)(2,1)} async-done(((bf16[256,1024]{1,0:T(8,128)(2,1)}), bf16[1024,1024]{1,0:T(8,128)(2,1)}) %all-gather.3.cloned.1.call-update) | async-done | bytes 2097168 | tf_op jit(solution)/shard_map/all_gather | solution.py:238
  57.3 0.0 copy-done
  57.3 23.0 %multiply_reduce_fusion.5 = (f32[704]{0:T(1024)S(1)}, f32[704]{0:T(1024)S(1)}, f32[704]{0:T(1024)S(1)}, f32[704]{0:T(1024)S(1)}, f32[704]{0:T(1024)S(1)}, /*inde...) fusion(bf16[1024,1408]{0,1:T(8,128)(2,1)} %copy-done.2, ...), kind=kOutput, calls=%fused_computation.28 | convolution fusion | flops 1501621760 | bytes 23757824 | tf_op jit(solution)/shard_map/dot_general | solution.py:45
  80.3 11.0 %fusion.5 = (bf16[1024,704]{0,1:T(8,128)(2,1)S(1)}, bf16[1024,704]{0,1:T(8,128)(2,1)S(1)}) fusion(f32[1024,704]{0,1:T(8,128)} %get-tuple-element.36, f32[704]{0:T(1024)S(1)} %get-tuple-element.34, f32[704]{0:T(1024)S(1)} %get-tuple-element.35, f32[704]{0:T(1024)S(1)} %get-tuple-element.33, f32[1024,704]{0,1:T(8,128)} %get-tuple-element.38, ...), kind=kLoop, calls=%fused_computation.15 | loop fusion | flops 8650752 | bytes 8667648 | tf_op jit(solution)/shard_map/convert_element_type | solution.py:250
  91.3 0.0 copy-start.4
  91.3 5.6 %convolution_convert_fusion.2.ig = bf16[1024,1024]{1,0:T(8,128)(2,1)S(1)} fusion(bf16[1024,1408]{0,1:T(8,128)(2,1)} %constant_dynamic-update-slice_fusion, bf16[1024,704]{0,1:T(8,128)(2,1)S(1)} %get-tuple-element.47, bf16[1024,704]{0,1:T(8,128)(2,1)S(1)} %get-tuple-element.46), kind=kOutput, calls=%fused_computation.35 | convolution fusion | flops 2959605760 | bytes 7864320 | tf_op jit(solution)/shard_map/dot_general | solution.py:45
  97.0 0.1 fusion.15.taps
  97.1 0.0 copy-done.4
  97.1 0.0 copy-start.5
  97.1 0.0 copy-start.6
  97.1 0.0 copy-start.7
  97.1 4.9 %fusion.1.gv = bf16[1024,1408]{1,0:T(8,128)(2,1)} fusion(bf16[1024,1024]{1,0:T(8,128)(2,1)S(1)} %copy-done.4, bf16[1024,704]{0,1:T(8,128)(2,1)S(1)} %get-tuple-element.47, bf16[1024,704]{0,1:T(8,128)(2,1)S(1)} %get-tuple-element.46), kind=kOutput, calls=%fused_computation.3 | convolution fusion | flops 2959998976 | bytes 7864320 | tf_op jit(solution)/shard_map/dot_general | solution.py:39
  102.0 0.0 copy-done.5
  102.0 0.0 copy-done.6
  102.0 0.0 copy-done.7
  102.0 1.7 convolution_convert_fusion.3.dn
  103.8 143.4 %shard_map.118 = (bf16[1024,1408]{1,0:T(8,128)(2,1)}, bf16[704,1024]{1,0:T(8,128)(2,1)S(1)}, bf16[256,1024]{1,0:T(8,128)(2,1)S(1)}, f32[8,1408]{1,0:T(8,128)S(1)}) custom-call(bf16[1024,1408]{1,0:T(8,128)(2,1)} %fusion.1.gv, bf16[704,1024]{1,0:T(8,128)(2,1)S(1)} %convolution_convert_fusion.3.dn, bf16[1024,1024]{1,0:T(8,128)(2,1)S(1)} %convolution_convert_fusion.2.ig, ...), custom_call_target="tpu_custom_call" | custom-call | tf_op jit(solution)/shard_map/pallas_call | solution.py:198
  247.2 0.0 copy-start.1
  247.2 0.7 fusion.20
  247.9 1.9 convert_element_type.72
  249.8 0.0 copy-done.1
  249.8 3.4 %slice_convert_fusion = (f32[1024,704]{1,0:T(8,128)}, f32[1024,704]{1,0:T(8,128)}) fusion(bf16[1024,1408]{1,0:T(8,128)(2,1)S(1)} %copy-done.1), kind=kLoop, calls=%fused_computation.37 | loop fusion | flops 1441792 | bytes 8650752 | tf_op jit(solution)/shard_map/convert_element_type | solution.py:266
  253.2 3.4 %copy.15 = f32[1024,704]{0,1:T(8,128)} copy(f32[1024,704]{1,0:T(8,128)} %get-tuple-element.40) | data formatting | bytes 5767168
  256.6 3.4 %copy.14 = f32[1024,704]{0,1:T(8,128)} copy(f32[1024,704]{1,0:T(8,128)} %get-tuple-element.41) | data formatting | bytes 5767168
  260.1 0.8 copy.19
  (6 shorter events, 0.0 us)
Async XLA Ops:
  7.2 50.1 %copy-start = (bf16[704,1024]{1,0:T(8,128)(2,1)S(1)}, bf16[704,1024]{1,0:T(8,128)(2,1)}, u32[]{:S(2)}) copy-start(bf16[704,1024]{1,0:T(8,128)(2,1)} %param.11) | copy-start | bytes 4325380
  7.2 5.8 %copy-start.3 = (bf16[1024,704]{0,1:T(8,128)(2,1)S(1)}, bf16[1024,704]{0,1:T(8,128)(2,1)}, u32[]{:S(2)}) copy-start(bf16[1024,704]{0,1:T(8,128)(2,1)} %param.10) | copy-start | bytes 4325380
  7.2 25.9 %all-gather.5.cloned.1.call-start = ((), (), s32[]{:S(2)}) async-start(), calls=%async_computation.1 | async-start | bytes 2621440 | tf_op jit(solution)/shard_map/all_gather | solution.py:233
  7.9 49.4 %all-gather.3.cloned.1.call-start = ((), (), s32[]{:S(2)}) async-start(), calls=%async_computation | async-start | bytes 2621440 | tf_op jit(solution)/shard_map/all_gather | solution.py:238
  38.8 1.6 copy-start.2
  91.3 5.8 %copy-start.4 = (bf16[1024,1024]{1,0:T(8,128)(2,1)S(1)}, bf16[1024,1024]{1,0:T(8,128)(2,1)}, u32[]{:S(2)}) copy-start(bf16[1024,1024]{1,0:T(8,128)(2,1)} %all-gather.5.cloned.1.call-done) | copy-start | bytes 6291460
  97.1 4.9 %copy-start.5 = (bf16[1024,1024]{1,0:T(8,128)(2,1)S(1)}, bf16[1024,1024]{1,0:T(8,128)(2,1)}, u32[]{:S(2)}) copy-start(bf16[1024,1024]{1,0:T(8,128)(2,1)} %all-gather.3.cloned.1.call-done) | copy-start | bytes 6291460
  97.1 4.9 %copy-start.6 = (f32[1024,704]{0,1:T(8,128)S(1)}, f32[1024,704]{0,1:T(8,128)}, u32[]{:S(2)}) copy-start(f32[1024,704]{0,1:T(8,128)} %get-tuple-element.37) | copy-start | bytes 8650756
  97.1 4.9 %copy-start.7 = (f32[1024,704]{0,1:T(8,128)S(1)}, f32[1024,704]{0,1:T(8,128)}, u32[]{:S(2)}) copy-start(f32[1024,704]{0,1:T(8,128)} %get-tuple-element.39) | copy-start | bytes 8650756
  247.2 2.6 copy-start.1
Sparse Core Ops, SparseCore 0:
  9.6 23.5 all-gather.4
  34.7 22.5 all-gather.2

commit v2 on v0

--- a/solution.py
+++ b/solution.py
@@ -1,8 +1,11 @@
+import functools
 import math
 
 import jax
 import jax.numpy as jnp
 from jax import lax
+from jax.experimental import pallas as pl
+from jax.experimental.pallas import tpu as pltpu
 from jax.sharding import PartitionSpec as P
 
 
@@ -41,6 +44,323 @@
 def contract_cols(left, right):
     return lax.dot_general(
         left, right, (((1,), (1,)), ((), ())), preferred_element_type=jnp.float32
+    )
+
+MESH = pl.DeviceIdType.MESH
+BF16 = jnp.bfloat16
+F32 = jnp.float32
+STRIP = 16
+HALO = 8
+
+
+def send(src, dst, send_sem, recv_sem, where):
+    return pltpu.make_async_remote_copy(
+        src_ref=src, dst_ref=dst, send_sem=send_sem, recv_sem=recv_sem, device_id=where, device_id_type=MESH
+    )
+
+
+def layer_kernel(
+    n, scale,
+    tok, cot, gw, vw, dw, gt, vt,
+    g_out, v_out, dn_out, ig_out, taps_out,
+    tok_all, cot_all, tok_t, hid, hid_t, up_g, up_v, bg, bv, gg, gv,
+    g_part, v_part, dn_part, ig_part, taps_acc, taps_mine,
+    g_y, v_y, dn_y, g_z, v_z, dn_z, g_in, v_in, dn_in, ig_in, taps_in,
+    tok_send, tok_recv, cot_send, cot_recv,
+    y_send, y_recv, z_send, z_recv, az_send, az_recv, ay_send, ay_recv, ig_send, ig_recv, t_send, t_recv,
+):
+    depth = n // 2
+    me = lax.axis_index("rep")
+    y, z = lax.rem(me, 2), lax.div(me, 2)
+    partner = me + 1 - 2 * y
+    my_fs, my_tp = lax.axis_index("fs"), lax.axis_index("tp")
+    local = tok.shape[0]
+    seq = 4 * local
+    hidden_cols = gw.shape[1]
+    count = gt.shape[0]
+    mine = my_fs * 2 + my_tp
+    core_spot = my_fs * 2 + 1 - my_tp
+    far_spot = (1 - my_fs) * 2 + my_tp
+    diag_spot = 3 - mine
+    core, far, diag = {"tp": 1 - my_tp}, {"fs": 1 - my_fs}, {"fs": 1 - my_fs, "tp": 1 - my_tp}
+
+    def shard(spot):
+        return pl.ds(pl.multiple_of(spot * local, local), local)
+
+    barrier = pltpu.get_barrier_semaphore()
+    for offset in range(1, n):
+        pl.semaphore_signal(barrier, inc=1, device_id={"rep": lax.rem(me + offset, n)}, device_id_type=MESH)
+    for where in (core, far, diag):
+        pl.semaphore_signal(barrier, inc=1, device_id=where, device_id_type=MESH)
+    pl.semaphore_wait(barrier, n - 1 + 3)
+
+    def gather(own, every, sends, recvs, slot, where):
+        c = send(own, every.at[shard(mine), :], sends.at[slot], recvs.at[slot], where)
+        c.start()
+        return c
+
+    def relay(every, sends, recvs):
+        part = every.at[shard(far_spot), :]
+        c = send(part, part, sends.at[2], recvs.at[2], core)
+        c.start()
+        return c
+
+    tok_far = gather(tok, tok_all, tok_send, tok_recv, 0, far)
+    tok_core = gather(tok, tok_all, tok_send, tok_recv, 1, core)
+    cot_core = gather(cot, cot_all, cot_send, cot_recv, 1, core)
+    tok_all[shard(mine), :] = tok[...]
+    cot_all[shard(mine), :] = cot[...]
+    zeros = jnp.zeros((HALO, hidden_cols), F32)
+    up_g[0:HALO, :] = zeros
+    up_v[0:HALO, :] = zeros
+    bg[seq:seq + HALO, :] = zeros
+    bv[seq:seq + HALO, :] = zeros
+    taps_acc[...] = jnp.zeros_like(taps_acc)
+
+    def project(spot):
+        part = tok_all[shard(spot), :]
+        rows = pl.ds(pl.multiple_of(spot * local + HALO, HALO), local)
+        up_g[rows, :] = jnp.dot(part, gw[...], preferred_element_type=F32).astype(BF16).astype(F32)
+        up_v[rows, :] = jnp.dot(part, vw[...], preferred_element_type=F32).astype(BF16).astype(F32)
+        tok_t[:, shard(spot)] = part.T
+
+    project(mine)
+    tok_core.wait_recv()
+    project(core_spot)
+    tok_far.wait_recv()
+    cot_far = gather(cot, cot_all, cot_send, cot_recv, 0, far)
+    tok_relay = relay(tok_all, tok_send, tok_recv)
+    project(far_spot)
+    tok_relay.wait_recv()
+    project(diag_spot)
+
+    def mix(i, carry):
+        start = pl.multiple_of(i * STRIP, STRIP)
+        gs = up_g[pl.ds(start, STRIP + HALO), :]
+        vs = up_v[pl.ds(start, STRIP + HALO), :]
+        conv_gate = gt[0:1, :] * gs[HALO:HALO + STRIP]
+        conv_value = vt[0:1, :] * vs[HALO:HALO + STRIP]
+        for k in range(1, count):
+            conv_gate = conv_gate + gt[k:k + 1, :] * gs[HALO - k:HALO - k + STRIP]
+            conv_value = conv_value + vt[k:k + 1, :] * vs[HALO - k:HALO - k + STRIP]
+        sigma = jax.nn.sigmoid(conv_gate)
+        silu = conv_gate * sigma
+        hid[pl.ds(start, STRIP), :] = (silu * conv_value).astype(BF16)
+        bv[pl.ds(start, STRIP), :] = silu
+        bg[pl.ds(start, STRIP), :] = conv_value * sigma * (1.0 + conv_gate * (1.0 - sigma))
+        return carry
+
+    lax.fori_loop(0, seq // STRIP, mix, 0)
+
+    def turn(i, carry):
+        rows = pl.ds(pl.multiple_of(i * local, local), local)
+        hid_t[:, rows] = hid[rows, :].T
+        return carry
+
+    lax.fori_loop(0, 4, turn, 0)
+
+    def pull_back(spot):
+        rows = shard(spot)
+        back = contract_cols(cot_all[rows, :], dw[...])
+        bv[rows, :] = back * bv[rows, :]
+        bg[rows, :] = back * bg[rows, :]
+
+    pull_back(mine)
+    cot_core.wait_recv()
+    pull_back(core_spot)
+    cot_far.wait_recv()
+    cot_relay = relay(cot_all, cot_send, cot_recv)
+    pull_back(far_spot)
+    cot_relay.wait_recv()
+
+    g_rows = g_part.shape[0] // n
+    d_cols = dn_part.shape[1] // n
+
+    def row_cut(chunk, width=1):
+        return (pl.ds(pl.multiple_of(chunk * g_rows, g_rows), g_rows * width), slice(None))
+
+    def col_cut(chunk, width=1):
+        return (slice(None), pl.ds(pl.multiple_of(chunk * d_cols, d_cols), d_cols * width))
+
+    order = list(range(1, depth)) + [0]
+    kinds = (
+        (0, col_cut, dn_part, dn_y, dn_z, dn_in, dn_out),
+        (1, row_cut, g_part, g_y, g_z, g_in, g_out),
+        (2, row_cut, v_part, v_y, v_z, v_in, v_out),
+    )
+    waits = []
+
+    def exchange(kind, k):
+        index, cut, part, slots = kind[:4]
+        theirs = 2 * lax.rem(z + k, depth) + 1 - y
+        c = send(part.at[cut(theirs)], slots.at[k], y_send.at[index, k], y_recv.at[index, k], {"rep": partner})
+        c.start()
+        waits.append(c)
+        return c
+
+    def first_stage(kind, product):
+        cut, part = kind[1], kind[2]
+        sent = {}
+        for k in order:
+            pair = cut(2 * lax.rem(z + k, depth), 2)
+            part[pair] = product(pair).astype(BF16)
+            sent[k] = exchange(kind, k)
+        return sent
+
+    def second_stage(kind, sent):
+        index, cut, part, slots, sums, arrivals = kind[:6]
+        passed = []
+        for k in order:
+            ours = 2 * lax.rem(z + k, depth) + y
+            sent[k].wait_recv()
+            sums[k] = (part[cut(ours)].astype(F32) + slots[k].astype(F32)).astype(BF16)
+            if k:
+                c = send(sums.at[k], arrivals.at[k], z_send.at[index, k], z_recv.at[index, k], {"rep": ours})
+                c.start()
+                waits.append(c)
+                passed.append(c)
+        return passed
+
+    def spread(kind, chunk, k, sends, recvs, where):
+        index, cut, out = kind[0], kind[1], kind[6]
+        c = send(out.at[cut(chunk)], out.at[cut(chunk)], sends.at[index, k], recvs.at[index, k], where)
+        c.start()
+        waits.append(c)
+        return c
+
+    def third_stage(kind, passed):
+        cut, sums, arrivals, out = kind[1], kind[4], kind[5], kind[6]
+        for c in passed:
+            c.wait_recv()
+        total = sums[0].astype(F32)
+        for k in range(1, depth):
+            total = total + arrivals[k].astype(F32)
+        out[cut(me)] = (total * scale).astype(BF16)
+        lines = [spread(kind, me, k, az_send, az_recv, {"rep": 2 * lax.rem(z + k, depth) + y}) for k in range(1, depth)]
+        return lines, [spread(kind, me, 0, ay_send, ay_recv, {"rep": partner})]
+
+    def fourth_stage(kind, lines, ends):
+        for k in range(1, depth):
+            lines[k - 1].wait_recv()
+            chunk = 2 * lax.rem(z + depth - k, depth) + y
+            ends.append(spread(kind, chunk, k, ay_send, ay_recv, {"rep": partner}))
+        return ends
+
+    pull_back(diag_spot)
+    dn_sent = first_stage(
+        kinds[0], lambda cut: jnp.dot(hid_t[...], cot_all[cut], preferred_element_type=F32)
+    )
+
+    def unmix(i, carry):
+        start = pl.multiple_of(i * STRIP, STRIP)
+        for slot, (field, back, taps, grad) in enumerate(((up_g, bg, gt, gg), (up_v, bv, vt, gv))):
+            fs_ = field[pl.ds(start, STRIP + HALO), :]
+            bs = back[pl.ds(start, STRIP + HALO), :]
+            now = bs[0:STRIP]
+            total = taps[0:1, :] * now
+            for k in range(1, count):
+                total = total + taps[k:k + 1, :] * bs[k:k + STRIP]
+            grad[pl.ds(start, STRIP), :] = total.astype(BF16)
+            for k in range(count):
+                term = now * fs_[HALO - k:HALO - k + STRIP]
+                taps_acc[slot * count + k] += term[0:8] + term[8:16]
+        return carry
+
+    lax.fori_loop(0, seq // STRIP, unmix, 0)
+    g_sent = first_stage(kinds[1], lambda cut: jnp.dot(tok_t[cut], gg[...], preferred_element_type=F32))
+    v_sent = first_stage(kinds[2], lambda cut: jnp.dot(tok_t[cut], gv[...], preferred_element_type=F32))
+
+    taps_mine[...] = jnp.sum(taps_acc[...], axis=1)
+    taps_sent = []
+    for offset in range(1, n):
+        c = send(
+            taps_mine, taps_in.at[me], t_send.at[offset - 1], t_recv.at[offset - 1],
+            {"rep": lax.rem(me + offset, n)},
+        )
+        c.start()
+        taps_sent.append(c)
+
+    dn_passed = second_stage(kinds[0], dn_sent)
+    ig_sent = []
+    for slot, (spot, where) in enumerate(((far_spot, far), (diag_spot, diag), (core_spot, core), (mine, None))):
+        rows = shard(spot)
+        ig_part[rows, :] = (contract_cols(gg[rows, :], gw[...]) + contract_cols(gv[rows, :], vw[...])).astype(BF16)
+        if where is not None:
+            c = send(ig_part.at[rows, :], ig_in.at[slot], ig_send.at[slot], ig_recv.at[slot], where)
+            c.start()
+            ig_sent.append(c)
+    dn_lines, dn_ends = third_stage(kinds[0], dn_passed)
+    g_passed = second_stage(kinds[1], g_sent)
+    dn_ends = fourth_stage(kinds[0], dn_lines, dn_ends)
+    g_lines, g_ends = third_stage(kinds[1], g_passed)
+    v_passed = second_stage(kinds[2], v_sent)
+    g_ends = fourth_stage(kinds[1], g_lines, g_ends)
+    v_lines, v_ends = third_stage(kinds[2], v_passed)
+
+    for c in ig_sent:
+        c.wait_recv()
+    own = ig_part[shard(mine), :].astype(F32)
+    for slot in range(3):
+        own = own + ig_in[slot].astype(F32)
+    ig_out[...] = own.astype(BF16)
+    for c in taps_sent:
+        c.wait_recv()
+    taps_in[me] = taps_mine[...]
+    total = taps_in[0]
+    for slot in range(1, n):
+        total = total + taps_in[slot]
+    taps_out[...] = total * scale
+
+    v_ends = fourth_stage(kinds[2], v_lines, v_ends)
+    for c in dn_ends + g_ends + v_ends:
+        c.wait_recv()
+    for c in waits + taps_sent + ig_sent + [tok_far, tok_core, tok_relay, cot_far, cot_core, cot_relay]:
+        c.wait_send()
+
+
+def whole_layer(tokens, cotangent, gate_weight, value_weight, down_weight, gate_taps, value_taps, n, scale):
+    depth = n // 2
+    local, model = tokens.shape
+    seq = 4 * local
+    cols = gate_weight.shape[1]
+    count = gate_taps.shape[0]
+    dma = pltpu.SemaphoreType.DMA
+    vmem = pl.BlockSpec(memory_space=pltpu.VMEM)
+    rows_slots = pltpu.VMEM((depth, model // n, cols), BF16)
+    cols_slots = pltpu.VMEM((depth, cols, model // n), BF16)
+    return pl.pallas_call(
+        functools.partial(layer_kernel, n, scale),
+        out_shape=(
+            jax.ShapeDtypeStruct((model, cols), BF16),
+            jax.ShapeDtypeStruct((model, cols), BF16),
+            jax.ShapeDtypeStruct((cols, model), BF16),
+            jax.ShapeDtypeStruct((local, model), BF16),
+            jax.ShapeDtypeStruct((2 * count, cols), F32),
+        ),
+        in_specs=[vmem] * 7,
+        out_specs=(vmem,) * 5,
+        scratch_shapes=[
+            pltpu.VMEM((seq, model), BF16), pltpu.VMEM((seq, model), BF16), pltpu.VMEM((model, seq), BF16),
+            pltpu.VMEM((seq, cols), BF16), pltpu.VMEM((cols, seq), BF16),
+            pltpu.VMEM((seq + HALO, cols), F32), pltpu.VMEM((seq + HALO, cols), F32),
+            pltpu.VMEM((seq + HALO, cols), F32), pltpu.VMEM((seq + HALO, cols), F32),
+            pltpu.VMEM((seq, cols), BF16), pltpu.VMEM((seq, cols), BF16),
+            pltpu.VMEM((model, cols), BF16), pltpu.VMEM((model, cols), BF16), pltpu.VMEM((cols, model), BF16),
+            pltpu.VMEM((seq, model), BF16),
+            pltpu.VMEM((2 * count, 8, cols), F32), pltpu.VMEM((2 * count, cols), F32),
+        ] + [rows_slots, rows_slots, cols_slots] * 3 + [
+            pltpu.VMEM((3, local, model), BF16), pltpu.VMEM((n, 2 * count, cols), F32),
+        ] + [dma((3,))] * 4 + [dma((3, depth))] * 8 + [dma((3,))] * 2 + [dma((n - 1,))] * 2,
+        compiler_params=pltpu.CompilerParams(
+            collective_id=0, has_side_effects=True, vmem_limit_bytes=60 * 1024 * 1024
+        ),
+    )(tokens, cotangent, gate_weight, value_weight, down_weight, gate_taps, value_taps)
+
+
+def tiles_well(n, fs, tp, local, model, cols):
+    return (
+        n % 2 == 0 and fs == 2 and tp == 2 and model % (128 * n) == 0 and cols % 16 == 0 and local % 128 == 0
+        and local * model <= 512 * 1024 and model * cols <= 1024 * 768
     )
 
 
@@ -50,6 +370,16 @@
     seq_len = local_rows * lax.axis_size("fs") * lax.axis_size("tp")
     total_tokens = seq_len * lax.axis_size("rep")
     scale = 1.0 / math.sqrt(total_tokens)
+    n, fs, tp = lax.axis_size("rep"), lax.axis_size("fs"), lax.axis_size("tp")
+    if tiles_well(n, fs, tp, local_rows, tokens.shape[1], hidden_cols):
+        gate, value, down, input_grad, taps = whole_layer(
+            tokens, cotangent, gate_weight, value_weight, down_weight, gate_taps, value_taps, n, scale
+        )
+        count = gate_taps.shape[0]
+        return (
+            input_grad, gate.astype(jnp.float32), value.astype(jnp.float32), down.astype(jnp.float32),
+            taps[:count], taps[count:],
+        )
     both_weights = jnp.concatenate([gate_weight, value_weight], axis=1)
     piece = lax.all_gather(tokens, ("fs", "tp"), axis=0, tiled=True)
     whole = piece

time: 441 us -> 182 us (0.41)
  waiting for transfers between devices: 312 us -> 0 us
  Pallas kernels: 0 us -> 167 us
  matrix products: 46.5 us -> 0 us
  blocking collectives: 32.5 us -> 0 us
  other arithmetic: 24.9 us -> 1.94 us
  between operations: 13.9 us -> 0.66 us
  local copies, waits for them, and re-layouts: 6.5 us -> 11.5 us
    psum x1 -> x0, waiting for transfers between devices: 274 us -> none  [per_device(): lax.psum((gate_part, value_part, down_part, gate_tap_part, value_tap_part...]
    pallas_call x0 -> x1, Pallas kernels: none -> 167 us  [whole_layer(): pl.pallas_call(functools.partial(layer_kernel, n, scale), out_shape=(jax....]
    dot_general x7 -> x0, matrix products: 46.5 us -> none  [the longest x3 29.3 us: contract_cols(): lax.dot_general(left, right, (((1,), (1,)), ((), ())), preferred_element_...]
    all_gather x2 -> x0, waiting for transfers between devices: 36.4 us -> none  [the longest x1 22.7 us: per_device(): piece = lax.all_gather(tokens, ('fs', 'tp'), axis=0, tiled=True)]
    psum x1 -> x0, blocking collectives: 32.5 us -> none  [per_device(): lax.psum((gate_part, value_part, down_part, gate_tap_part, value_tap_part...]
    convert_element_type x3 -> x1, other arithmetic: 16.3 us -> 1.94 us  [per_device(): down.astype(jnp.float32)]
    mul x4 -> x0, other arithmetic: 8.52 us -> none  [per_device(): weight_out = tuple((item * scale for item in summed))]
    unnamed x22 -> x13, local copies, waits for them, and re-layouts: 4.78 us -> 10.1 us
  transfers between devices with their start and end apart: 4 -> 0, of which waited for: 3 -> 0; matrix products, arithmetic and copies ran while one was open for 6% -> 0% of each run, Pallas kernels for 0% -> 0%
where the time goes in v2:
time: 182 us; the launch traced here: 181 us
  Pallas kernels  167 us (92%)
  local copies, waits for them, and re-layouts  11.5 us (6%)
  other arithmetic  1.94 us (1%)
    pallas_call x1, Pallas kernels, whole_layer(): pl.pallas_call(functools.partial(layer_kernel, n, scale), out_shape=(jax....  167 us
    unnamed x13, local copies, waits for them, and re-layouts  10.1 us

profile of v2, /device:TPU:24, one launch (start us, length us, event | category | flops | bytes accessed | tf_op | source)
XLA Modules:
  0.0 181.2 jit_solution(3750341513695012063)
XLA Ops:
  0.6 0.0 copy-start.1
  0.6 2.7 %copy.13.gw = bf16[1024,704]{1,0:T(8,128)(2,1)} copy(bf16[1024,704]{0,1:T(8,128)(2,1)} %param.9) | data formatting | bytes 2883584 | tf_op args[2]
  3.3 0.0 copy-done.1
  3.3 1.6 copy.14.vw
  4.9 167.1 %shard_map.118 = (bf16[1024,704]{1,0:T(8,128)(2,1)}, bf16[1024,704]{1,0:T(8,128)(2,1)}, bf16[704,1024]{1,0:T(8,128)(2,1)}, bf16[256,1024]{1,0:T(8,128)(2,1)}, f32[6,704]{1,0:T(8,128)}) custom-call(bf16[256,1024]{1,0:T(8,128)(2,1)} %tok.1, bf16[256,1024]{1,0:T(8,128)(2,1)} %cot.1, bf16[1024,704]{1,0:T(8,128)(2,1)} %copy.13.gw, bf16[1024,704]{1,0:T(8,128)(2,1)} %copy.14.vw, ...), custom_call_target="tpu_custom_call" | custom-call | tf_op jit(solution)/shard_map/pallas_call | solution.py:331
  172.0 1.4 fusion
  173.4 0.0 copy-start
  173.4 3.1 %copy.15 = f32[1024,704]{0,1:T(8,128)} copy(bf16[1024,704]{1,0:T(8,128)(2,1)} %get-tuple-element.12) | data formatting | bytes 4325376
  176.5 0.0 copy-done
  176.5 0.0 copy-start.2
  176.5 2.0 %copy.16 = f32[1024,704]{0,1:T(8,128)} copy(bf16[1024,704]{1,0:T(8,128)(2,1)S(1)} %copy-done) | data formatting | bytes 4325376
  178.4 0.0 copy-done.2
  178.4 0.0 copy-start.3
  178.4 1.9 %convert_element_type.11 = f32[704,1024]{1,0:T(8,128)} convert(bf16[704,1024]{1,0:T(8,128)(2,1)S(1)} %copy-done.2) | non-fusion elementwise | flops 720896 | bytes 4325376 | tf_op jit(solution)/shard_map/convert_element_type | solution.py:380
  180.4 0.0 copy-done.3
  180.4 0.8 copy.18
Async XLA Ops:
  0.6 2.7 %copy-start.1 = (bf16[1024,704]{0,1:T(8,128)(2,1)S(1)}, bf16[1024,704]{0,1:T(8,128)(2,1)}, u32[]{:S(2)}) copy-start(bf16[1024,704]{0,1:T(8,128)(2,1)} %param.10) | copy-start | bytes 4325380
  173.4 3.1 %copy-start = (bf16[1024,704]{1,0:T(8,128)(2,1)S(1)}, bf16[1024,704]{1,0:T(8,128)(2,1)}, u32[]{:S(2)}) copy-start(bf16[1024,704]{1,0:T(8,128)(2,1)} %get-tuple-element.13) | copy-start | bytes 4325380
  176.5 2.0 %copy-start.2 = (bf16[704,1024]{1,0:T(8,128)(2,1)S(1)}, bf16[704,1024]{1,0:T(8,128)(2,1)}, u32[]{:S(2)}) copy-start(bf16[704,1024]{1,0:T(8,128)(2,1)} %get-tuple-element.14) | copy-start | bytes 4325380
  178.4 1.9 %copy-start.3 = (bf16[256,1024]{1,0:T(8,128)(2,1)S(1)}, bf16[256,1024]{1,0:T(8,128)(2,1)}, u32[]{:S(2)}) copy-start(bf16[256,1024]{1,0:T(8,128)(2,1)} %get-tuple-element.30) | copy-start | bytes 1572868

commit v3 on v2

--- a/solution.py
+++ b/solution.py
@@ -63,7 +63,7 @@
     n, scale,
     tok, cot, gw, vw, dw, gt, vt,
     g_out, v_out, dn_out, ig_out, taps_out,
-    tok_all, cot_all, tok_t, hid, hid_t, up_g, up_v, bg, bv, gg, gv,
+    tok_all, cot_all, hid, hid_t, up_g, up_v, bg, bv, gg, gv, gg_t, gv_t,
     g_part, v_part, dn_part, ig_part, taps_acc, taps_mine,
     g_y, v_y, dn_y, g_z, v_z, dn_z, g_in, v_in, dn_in, ig_in, taps_in,
     tok_send, tok_recv, cot_send, cot_recv,
@@ -76,7 +76,7 @@
     my_fs, my_tp = lax.axis_index("fs"), lax.axis_index("tp")
     local = tok.shape[0]
     seq = 4 * local
-    hidden_cols = gw.shape[1]
+    hidden_cols = gw.shape[0]
     count = gt.shape[0]
     mine = my_fs * 2 + my_tp
     core_spot = my_fs * 2 + 1 - my_tp
@@ -120,9 +120,8 @@
     def project(spot):
         part = tok_all[shard(spot), :]
         rows = pl.ds(pl.multiple_of(spot * local + HALO, HALO), local)
-        up_g[rows, :] = jnp.dot(part, gw[...], preferred_element_type=F32).astype(BF16).astype(F32)
-        up_v[rows, :] = jnp.dot(part, vw[...], preferred_element_type=F32).astype(BF16).astype(F32)
-        tok_t[:, shard(spot)] = part.T
+        up_g[rows, :] = contract_cols(part, gw[...]).astype(BF16).astype(F32)
+        up_v[rows, :] = contract_cols(part, vw[...]).astype(BF16).astype(F32)
 
     project(mine)
     tok_core.wait_recv()
@@ -152,12 +151,16 @@
 
     lax.fori_loop(0, seq // STRIP, mix, 0)
 
-    def turn(i, carry):
-        rows = pl.ds(pl.multiple_of(i * local, local), local)
-        hid_t[:, rows] = hid[rows, :].T
-        return carry
-
-    lax.fori_loop(0, 4, turn, 0)
+    def turn(pairs):
+        def step(i, carry):
+            rows = pl.ds(pl.multiple_of(i * local, local), local)
+            for flat, tall in pairs:
+                tall[:, rows] = flat[rows, :].T
+            return carry
+
+        lax.fori_loop(0, 4, step, 0)
+
+    turn(((hid, hid_t),))
 
     def pull_back(spot):
         rows = shard(spot)
@@ -173,11 +176,7 @@
     pull_back(far_spot)
     cot_relay.wait_recv()
 
-    g_rows = g_part.shape[0] // n
     d_cols = dn_part.shape[1] // n
-
-    def row_cut(chunk, width=1):
-        return (pl.ds(pl.multiple_of(chunk * g_rows, g_rows), g_rows * width), slice(None))
 
     def col_cut(chunk, width=1):
         return (slice(None), pl.ds(pl.multiple_of(chunk * d_cols, d_cols), d_cols * width))
@@ -185,8 +184,8 @@
     order = list(range(1, depth)) + [0]
     kinds = (
         (0, col_cut, dn_part, dn_y, dn_z, dn_in, dn_out),
-        (1, row_cut, g_part, g_y, g_z, g_in, g_out),
-        (2, row_cut, v_part, v_y, v_z, v_in, v_out),
+        (1, col_cut, g_part, g_y, g_z, g_in, g_out),
+        (2, col_cut, v_part, v_y, v_z, v_in, v_out),
     )
     waits = []
 
@@ -267,8 +266,9 @@
         return carry
 
     lax.fori_loop(0, seq // STRIP, unmix, 0)
-    g_sent = first_stage(kinds[1], lambda cut: jnp.dot(tok_t[cut], gg[...], preferred_element_type=F32))
-    v_sent = first_stage(kinds[2], lambda cut: jnp.dot(tok_t[cut], gv[...], preferred_element_type=F32))
+    turn(((gg, gg_t), (gv, gv_t)))
+    g_sent = first_stage(kinds[1], lambda cut: jnp.dot(gg_t[...], tok_all[cut], preferred_element_type=F32))
+    v_sent = first_stage(kinds[2], lambda cut: jnp.dot(gv_t[...], tok_all[cut], preferred_element_type=F32))
 
     taps_mine[...] = jnp.sum(taps_acc[...], axis=1)
     taps_sent = []
@@ -284,7 +284,10 @@
     ig_sent = []
     for slot, (spot, where) in enumerate(((far_spot, far), (diag_spot, diag), (core_spot, core), (mine, None))):
         rows = shard(spot)
-        ig_part[rows, :] = (contract_cols(gg[rows, :], gw[...]) + contract_cols(gv[rows, :], vw[...])).astype(BF16)
+        ig_part[rows, :] = (
+            jnp.dot(gg[rows, :], gw[...], preferred_element_type=F32)
+            + jnp.dot(gv[rows, :], vw[...], preferred_element_type=F32)
+        ).astype(BF16)
         if where is not None:
             c = send(ig_part.at[rows, :], ig_in.at[slot], ig_send.at[slot], ig_recv.at[slot], where)
             c.start()
@@ -322,17 +325,16 @@
     depth = n // 2
     local, model = tokens.shape
     seq = 4 * local
-    cols = gate_weight.shape[1]
+    cols = gate_weight.shape[0]
     count = gate_taps.shape[0]
     dma = pltpu.SemaphoreType.DMA
     vmem = pl.BlockSpec(memory_space=pltpu.VMEM)
-    rows_slots = pltpu.VMEM((depth, model // n, cols), BF16)
     cols_slots = pltpu.VMEM((depth, cols, model // n), BF16)
     return pl.pallas_call(
         functools.partial(layer_kernel, n, scale),
         out_shape=(
-            jax.ShapeDtypeStruct((model, cols), BF16),
-            jax.ShapeDtypeStruct((model, cols), BF16),
+            jax.ShapeDtypeStruct((cols, model), BF16),
+            jax.ShapeDtypeStruct((cols, model), BF16),
             jax.ShapeDtypeStruct((cols, model), BF16),
             jax.ShapeDtypeStruct((local, model), BF16),
             jax.ShapeDtypeStruct((2 * count, cols), F32),
@@ -340,15 +342,16 @@
         in_specs=[vmem] * 7,
         out_specs=(vmem,) * 5,
         scratch_shapes=[
-            pltpu.VMEM((seq, model), BF16), pltpu.VMEM((seq, model), BF16), pltpu.VMEM((model, seq), BF16),
+            pltpu.VMEM((seq, model), BF16), pltpu.VMEM((seq, model), BF16),
             pltpu.VMEM((seq, cols), BF16), pltpu.VMEM((cols, seq), BF16),
             pltpu.VMEM((seq + HALO, cols), F32), pltpu.VMEM((seq + HALO, cols), F32),
             pltpu.VMEM((seq + HALO, cols), F32), pltpu.VMEM((seq + HALO, cols), F32),
             pltpu.VMEM((seq, cols), BF16), pltpu.VMEM((seq, cols), BF16),
-            pltpu.VMEM((model, cols), BF16), pltpu.VMEM((model, cols), BF16), pltpu.VMEM((cols, model), BF16),
+            pltpu.VMEM((cols, seq), BF16), pltpu.VMEM((cols, seq), BF16),
+            pltpu.VMEM((cols, model), BF16), pltpu.VMEM((cols, model), BF16), pltpu.VMEM((cols, model), BF16),
             pltpu.VMEM((seq, model), BF16),
             pltpu.VMEM((2 * count, 8, cols), F32), pltpu.VMEM((2 * count, cols), F32),
-        ] + [rows_slots, rows_slots, cols_slots] * 3 + [
+        ] + [cols_slots] * 9 + [
             pltpu.VMEM((3, local, model), BF16), pltpu.VMEM((n, 2 * count, cols), F32),
         ] + [dma((3,))] * 4 + [dma((3, depth))] * 8 + [dma((3,))] * 2 + [dma((n - 1,))] * 2,
         compiler_params=pltpu.CompilerParams(
@@ -373,11 +376,11 @@
     n, fs, tp = lax.axis_size("rep"), lax.axis_size("fs"), lax.axis_size("tp")
     if tiles_well(n, fs, tp, local_rows, tokens.shape[1], hidden_cols):
         gate, value, down, input_grad, taps = whole_layer(
-            tokens, cotangent, gate_weight, value_weight, down_weight, gate_taps, value_taps, n, scale
+            tokens, cotangent, gate_weight.T, value_weight.T, down_weight, gate_taps, value_taps, n, scale
         )
         count = gate_taps.shape[0]
         return (
-            input_grad, gate.astype(jnp.float32), value.astype(jnp.float32), down.astype(jnp.float32),
+            input_grad, gate.astype(jnp.float32).T, value.astype(jnp.float32).T, down.astype(jnp.float32),
             taps[:count], taps[count:],
         )
     both_weights = jnp.concatenate([gate_weight, value_weight], axis=1)

time: 182 us -> 175 us (0.962); the launches traced: 181 us -> 172 us
  local copies, waits for them, and re-layouts: 11.5 us -> 1.41 us
  other arithmetic: 1.94 us -> 7.08 us
  Pallas kernels: 167 us -> 163 us
    unnamed x13 -> x7, local copies, waits for them, and re-layouts: 10.1 us -> 0.81 us
    transpose x0 -> x1, other arithmetic: none -> 5.14 us  [per_device(): value.astype(jnp.float32)]
    pallas_call x1, Pallas kernels: 167 us -> 163 us  [whole_layer(): pl.pallas_call(functools.partial(layer_kernel, n, scale), out_shape=(jax....]
where the time goes in v3:
time: 175 us; the launch traced here: 172 us
  Pallas kernels  163 us (93%)
  other arithmetic  7.08 us (4%)
    pallas_call x1, Pallas kernels, whole_layer(): pl.pallas_call(functools.partial(layer_kernel, n, scale), out_shape=(jax....  163 us
    transpose x1, other arithmetic, per_device(): value.astype(jnp.float32)  5.14 us

profile of v3, /device:TPU:24, one launch (start us, length us, event | category | flops | bytes accessed | tf_op | source)
XLA Modules:
  0.0 172.2 jit_solution(3838516913606156626)
XLA Ops:
  0.6 163.1 %shard_map.118 = (bf16[704,1024]{1,0:T(8,128)(2,1)}, bf16[704,1024]{1,0:T(8,128)(2,1)}, bf16[704,1024]{1,0:T(8,128)(2,1)}, bf16[256,1024]{1,0:T(8,128)(2,1)}, f32[6,704]{1,0:T(8,128)}) custom-call(bf16[256,1024]{1,0:T(8,128)(2,1)} %tok.1, bf16[256,1024]{1,0:T(8,128)(2,1)} %cot.1, bf16[704,1024]{1,0:T(8,128)(2,1)} %bitcast.6, bf16[704,1024]{1,0:T(8,128)(2,1)} %bitcast.7, ...), custom_call_target="tpu_custom_call" | custom-call | tf_op jit(solution)/shard_map/pallas_call | solution.py:333
  163.7 0.0 copy-start.2
  163.7 0.0 copy-start
  163.7 5.1 %convert_bitcast_fusion = (f32[1024,704]{0,1:T(8,128)}, f32[1024,704]{0,1:T(8,128)}) fusion(bf16[704,1024]{1,0:T(8,128)(2,1)} %get-tuple-element.13, bf16[704,1024]{1,0:T(8,128)(2,1)} %get-tuple-element.12), kind=kLoop, calls=%fused_computation | loop fusion | flops 1441792 | bytes 8650752 | tf_op jit(solution)/shard_map/transpose | solution.py:383
  168.9 0.0 copy-done.2
  168.9 0.6 fusion
  169.5 0.0 copy-done
  169.5 0.0 copy-start.1
  169.5 1.9 %convert_element_type.2 = f32[704,1024]{1,0:T(8,128)} convert(bf16[704,1024]{1,0:T(8,128)(2,1)S(1)} %copy-done) | non-fusion elementwise | flops 720896 | bytes 4325376 | tf_op jit(solution)/shard_map/convert_element_type | solution.py:383
  171.4 0.0 copy-done.1
  171.4 0.8 copy.14
Async XLA Ops:
  163.7 5.2 %copy-start.2 = (f32[6,704]{1,0:T(8,128)S(1)}, f32[6,704]{1,0:T(8,128)}, u32[]{:S(2)}) copy-start(f32[6,704]{1,0:T(8,128)} %get-tuple-element.15) | copy-start | bytes 50692
  163.7 5.8 %copy-start = (bf16[704,1024]{1,0:T(8,128)(2,1)S(1)}, bf16[704,1024]{1,0:T(8,128)(2,1)}, u32[]{:S(2)}) copy-start(bf16[704,1024]{1,0:T(8,128)(2,1)} %get-tuple-element.14) | copy-start | bytes 4325380
  169.5 1.9 %copy-start.1 = (bf16[256,1024]{1,0:T(8,128)(2,1)S(1)}, bf16[256,1024]{1,0:T(8,128)(2,1)}, u32[]{:S(2)}) copy-start(bf16[256,1024]{1,0:T(8,128)(2,1)} %get-tuple-element.26) | copy-start | bytes 1572868

commit v4 on v3

--- a/solution.py
+++ b/solution.py
@@ -292,11 +292,11 @@
             c = send(ig_part.at[rows, :], ig_in.at[slot], ig_send.at[slot], ig_recv.at[slot], where)
             c.start()
             ig_sent.append(c)
+    g_passed = second_stage(kinds[1], g_sent)
     dn_lines, dn_ends = third_stage(kinds[0], dn_passed)
-    g_passed = second_stage(kinds[1], g_sent)
+    v_passed = second_stage(kinds[2], v_sent)
+    g_lines, g_ends = third_stage(kinds[1], g_passed)
     dn_ends = fourth_stage(kinds[0], dn_lines, dn_ends)
-    g_lines, g_ends = third_stage(kinds[1], g_passed)
-    v_passed = second_stage(kinds[2], v_sent)
     g_ends = fourth_stage(kinds[1], g_lines, g_ends)
     v_lines, v_ends = third_stage(kinds[2], v_passed)
 

time: 175 us -> 173 us (0.989); the launches traced: 172 us -> 172 us
  no operation moved by 1% of the time
where the time goes in v4:
time: 173 us; the launch traced here: 172 us
  Pallas kernels  163 us (94%)
  other arithmetic  7.08 us (4%)
    pallas_call x1, Pallas kernels, whole_layer(): pl.pallas_call(functools.partial(layer_kernel, n, scale), out_shape=(jax....  163 us
    transpose x1, other arithmetic, per_device(): value.astype(jnp.float32)  5.14 us

profile of v4, /device:TPU:24, one launch (start us, length us, event | category | flops | bytes accessed | tf_op | source)
XLA Modules:
  0.0 172.2 jit_solution(2836129506953120032)
XLA Ops:
  0.6 163.0 %shard_map.118 = (bf16[704,1024]{1,0:T(8,128)(2,1)}, bf16[704,1024]{1,0:T(8,128)(2,1)}, bf16[704,1024]{1,0:T(8,128)(2,1)}, bf16[256,1024]{1,0:T(8,128)(2,1)}, f32[6,704]{1,0:T(8,128)}) custom-call(bf16[256,1024]{1,0:T(8,128)(2,1)} %tok.1, bf16[256,1024]{1,0:T(8,128)(2,1)} %cot.1, bf16[704,1024]{1,0:T(8,128)(2,1)} %bitcast.6, bf16[704,1024]{1,0:T(8,128)(2,1)} %bitcast.7, ...), custom_call_target="tpu_custom_call" | custom-call | tf_op jit(solution)/shard_map/pallas_call | solution.py:333
  163.6 0.0 copy-start.2
  163.7 0.0 copy-start
  163.7 5.1 %convert_bitcast_fusion = (f32[1024,704]{0,1:T(8,128)}, f32[1024,704]{0,1:T(8,128)}) fusion(bf16[704,1024]{1,0:T(8,128)(2,1)} %get-tuple-element.13, bf16[704,1024]{1,0:T(8,128)(2,1)} %get-tuple-element.12), kind=kLoop, calls=%fused_computation | loop fusion | flops 1441792 | bytes 8650752 | tf_op jit(solution)/shard_map/transpose | solution.py:383
  168.8 0.0 copy-done.2
  168.8 0.6 fusion
  169.4 0.0 copy-done
  169.4 0.0 copy-start.1
  169.4 1.9 %convert_element_type.2 = f32[704,1024]{1,0:T(8,128)} convert(bf16[704,1024]{1,0:T(8,128)(2,1)S(1)} %copy-done) | non-fusion elementwise | flops 720896 | bytes 4325376 | tf_op jit(solution)/shard_map/convert_element_type | solution.py:383
  171.4 0.0 copy-done.1
  171.4 0.8 copy.14
Async XLA Ops:
  163.6 5.2 %copy-start.2 = (f32[6,704]{1,0:T(8,128)S(1)}, f32[6,704]{1,0:T(8,128)}, u32[]{:S(2)}) copy-start(f32[6,704]{1,0:T(8,128)} %get-tuple-element.15) | copy-start | bytes 50692
  163.7 5.8 %copy-start = (bf16[704,1024]{1,0:T(8,128)(2,1)S(1)}, bf16[704,1024]{1,0:T(8,128)(2,1)}, u32[]{:S(2)}) copy-start(bf16[704,1024]{1,0:T(8,128)(2,1)} %get-tuple-element.14) | copy-start | bytes 4325380
  169.4 1.9 %copy-start.1 = (bf16[256,1024]{1,0:T(8,128)(2,1)S(1)}, bf16[256,1024]{1,0:T(8,128)(2,1)}, u32[]{:S(2)}) copy-start(bf16[256,1024]{1,0:T(8,128)(2,1)} %get-tuple-element.26) | copy-start | bytes 1572868
